TPU v7x, 32 devices: a whole 2x2x4 slice. The times are simulated.
32 devices in a mesh: sp: 4 (over z), fs: 4 (over y, x), tp: 2 (over core).
Axes of the slice: x: 2, y: 2, z: 4, core: 2. Of those that a mesh axis runs over, the one named last changes fastest.
Arguments:
- tokens: bfloat16 [8192, 2048], P(('fs', 'sp')), parts along dimension 0, may hold values from -6 to 6
- norm_gain: bfloat16 [2048], replicated, may hold values from 0.099609375 to 1.8984375
- w_query: bfloat16 [2048, 1024], P('sp', 'tp'), may hold values from -0.15625 to 0.15625
- w_key: bfloat16 [2048, 256], P('sp', 'tp'), may hold values from -0.15625 to 0.15625
- w_value: bfloat16 [2048, 256], P('sp', 'tp'), may hold values from -0.125 to 0.125
- w_glu_value: bfloat16 [2048, 1024], P('sp', 'tp'), may hold values from -0.22097087 to 0.22097087
- w_glu_gate: bfloat16 [2048, 1024], P('sp', 'tp'), may hold values from -0.125 to 0.125
- conv_taps: bfloat16 [31, 1024], P(None, 'tp'), may hold values from -1 to 1
- convolution_norm_gain: bfloat16 [1024], replicated, may hold values from 0.099609375 to 1.8984375
- head_gain: bfloat16 [128], replicated, may hold values from 0.099609375 to 1.8984375
- lam: float32 [8], P('tp'), may hold values from 0.3 to 0.8
- w_out: bfloat16 [2048, 2048], P(None, 'sp'), may hold values from -0.125 to 0.125
Outputs:
- mixed: bfloat16 [8192, 2048], P(('fs', 'sp', 'tp')), parts along dimension 0
- log_totals: float32 [8192, 16], P(('fs', 'sp'), 'tp'), parts along dimension 0
There are 4 independent parts, one for each index of `fs`. A program takes and returns all parts, laid end to end along the dimension named above; an argument that names none is the same for every part. Nothing has to cross between parts.
All inputs are finite; a program needn't handle non-finite values.
Results may differ from a plain program's by a relative error of at most 0.0095.
Values may be sent and summed in bfloat16 or wider, within the bound.
A program may use at most 64 MiB of HBM per device.

v0:
```python
import functools
import math

import jax
import jax.numpy as jnp
from jax import lax
from jax.experimental import pallas as pl
from jax.experimental.pallas import tpu as pltpu
from jax.sharding import PartitionSpec as P

QK = 64
VDIM = 128
EPS = 1e-06
MESH = pl.DeviceIdType.MESH
BF = jnp.bfloat16
F32 = jnp.float32
LANES = 128
RIM = 32


def kernel(
    n,
    conv_total,
    tok_h,
    gain_r,
    wq_h,
    wk_h,
    wv_h,
    wgv_h,
    wgg_h,
    taps_r,
    cgain_r,
    hgain_r,
    lam_r,
    wo_h,
    mixed_r,
    log_r,
    tok,
    normed,
    gkv,
    gq,
    gb,
    gc,
    q2,
    kbuf,
    vbuf,
    acc,
    gated,
    rim,
    pad,
    conv,
    sq_own,
    sq_in,
    both,
    part_out,
    part_in,
    keep,
    loc,
    zs,
    zr,
    xs,
    xr,
    ys,
    yr,
    hxs,
    hxr,
    hys,
    hyr,
    kvs,
    kvr,
    rims,
    sqs,
    ps,
    pr,
):
    s = lax.axis_index("sp")
    f = lax.axis_index("fs")
    t = lax.axis_index("tp")
    fx = f + 1 - 2 * (f % 2)
    fy = (f + 2) % 4
    left = {"sp": s - 1, "fs": f, "tp": t}
    right = {"sp": s + 1, "fs": f, "tp": t}
    xdev = {"sp": s, "fs": fx, "tp": t}
    ydev = {"sp": s, "fs": fy, "tp": t}
    mate = {"sp": s, "fs": f, "tp": 1 - t}
    rows, width = tok.shape
    heads = lam_r.shape[0]
    chans = gated.shape[1]
    qcols = wq_h.shape[1]
    half = rows // 2
    groups = (gkv, gq, gb, gc)
    has_left = s > 0
    has_right = s < n - 1

    d_rows = wq_h.shape[0]
    att_rows = heads * VDIM
    locals_ = [
        (wk_h, gkv.at[s, :, pl.ds(0, LANES)]),
        (wv_h, gkv.at[s, :, pl.ds(LANES, LANES)]),
        (wq_h, gq.at[s]),
        (tok_h, tok),
        (wgv_h, gb.at[s, :, pl.ds(0, chans)]),
        (wgg_h, gb.at[s, :, pl.ds(chans, chans)]),
        (wo_h.at[pl.ds(t * att_rows, att_rows), :], gc.at[s, pl.ds(0, att_rows), :]),
        (
            wo_h.at[pl.ds(2 * att_rows + t * chans, chans), :],
            gc.at[s, pl.ds(att_rows, chans), :],
        ),
    ]
    copies = [pltpu.make_async_copy(a, b, loc.at[i]) for i, (a, b) in enumerate(locals_)]
    for c in copies:
        c.start()

    bar = pltpu.get_barrier_semaphore()
    for dev in (xdev, ydev, mate):
        pl.semaphore_signal(bar, 1, device_id=dev, device_id_type=MESH)

    @pl.when(has_left)
    def _():
        pl.semaphore_signal(bar, 1, device_id=left, device_id_type=MESH)

    @pl.when(has_right)
    def _():
        pl.semaphore_signal(bar, 1, device_id=right, device_id_type=MESH)

    pl.semaphore_wait(bar, 3 + jnp.where(has_left, 1, 0) + jnp.where(has_right, 1, 0))

    def chunk(g, o, q, part=None):
        buf = groups[g]
        size = buf.shape[1] // 4
        if part is None:
            return buf.at[o, pl.ds(pl.multiple_of(q * size, size), size), :]
        size = size // 2
        return buf.at[o, pl.ds(pl.multiple_of((q * 2 + part) * size, size), size), :]

    def zcopy(g, o, right_way):
        c = chunk(g, o, f)
        return pltpu.make_async_remote_copy(
            c,
            c,
            zs.at[g, 0 if right_way else 1, o],
            zr.at[g, o],
            device_id=right if right_way else left,
            device_id_type=MESH,
        )

    def xcopy(g, o, q):
        c = chunk(g, o, q)
        return pltpu.make_async_remote_copy(
            c, c, xs.at[g, o], xr.at[g, o], device_id=xdev, device_id_type=MESH
        )

    def ycopy(g, o, q):
        c = chunk(g, o, q)
        return pltpu.make_async_remote_copy(
            c, c, ys.at[g, o], yr.at[g, o], device_id=ydev, device_id_type=MESH
        )

    def hxcopy(g, o, q):
        c = chunk(g, o, q, 0)
        return pltpu.make_async_remote_copy(
            c, c, hxs.at[g, o], hxr.at[g, o], device_id=xdev, device_id_type=MESH
        )

    def hycopy(g, o, q):
        c = chunk(g, o, q, 1)
        return pltpu.make_async_remote_copy(
            c, c, hys.at[g, o], hyr.at[g, o], device_id=ydev, device_id_type=MESH
        )

    fd = 3 - f

    def sides(k, fn):
        @pl.when(s >= k)
        def _():
            fn(s - k, True)

        @pl.when(s + k < n)
        def _():
            fn(s + k, False)

    def own_send(g):
        @pl.when(has_right)
        def _():
            zcopy(g, s, True).start()

        @pl.when(has_left)
        def _():
            zcopy(g, s, False).start()

    def stage1(g, k):
        def go(o, right_way):
            zcopy(g, o, right_way).wait_recv()
            xcopy(g, o, f).start()
            ycopy(g, o, f).start()

            @pl.when(has_right if right_way else has_left)
            def _():
                zcopy(g, o, right_way).start()

        sides(k, go)

    def stage2(g, k):
        def go(o, right_way):
            xcopy(g, o, fx).wait_recv()
            hycopy(g, o, fx).start()
            ycopy(g, o, fy).wait_recv()
            hxcopy(g, o, fy).start()

        sides(k, go)

    def stage3(g, k):
        def go(o, right_way):
            hxcopy(g, o, fd).wait_recv()
            hycopy(g, o, fd).wait_recv()

        sides(k, go)

    def drain(g):
        own = zcopy(g, s, True)

        @pl.when(has_right)
        def _():
            own.wait_send()

        @pl.when(has_left)
        def _():
            zcopy(g, s, False).wait_send()

        for k in range(1, n):

            def go(o, right_way):
                xcopy(g, o, f).wait_send()
                ycopy(g, o, f).wait_send()
                hycopy(g, o, fx).wait_send()
                hxcopy(g, o, fy).wait_send()

                @pl.when(has_right if right_way else has_left)
                def _():
                    zcopy(g, o, right_way).wait_send()

            sides(k, go)

    def kvcopy(o):
        return [
            pltpu.make_async_remote_copy(
                b.at[o], b.at[o], kvs.at[i, o], kvr.at[i, o], device_id=right, device_id_type=MESH
            )
            for i, b in enumerate((kbuf, vbuf))
        ]

    def kv_take(k):
        @pl.when(s >= k)
        def _():
            for c in kvcopy(s - k):
                c.wait_recv()

            @pl.when(has_right)
            def _():
                for c in kvcopy(s - k):
                    c.start()

    tall = min(256, rows)
    per_head = 2 * rows // tall

    def attend(o, diagonal):
        vx = jnp.concatenate([vbuf[o], jnp.ones((rows, VDIM), BF)], axis=1)
        kx = kbuf[o]

        def step(i, carry):
            h = i // per_head
            at = pl.multiple_of((i % per_head) * tall, tall)
            score = lax.dot_general(
                q2[h, pl.ds(at, tall), :],
                kx,
                (((1,), (1,)), ((), ())),
                preferred_element_type=F32,
            )
            w = jnp.exp2(score * (QK**-0.5 * math.log2(math.e)))
            if diagonal:
                pos = (at % rows) + lax.broadcasted_iota(jnp.int32, w.shape, 0)
                w = jnp.where(lax.broadcasted_iota(jnp.int32, w.shape, 1) <= pos, w, 0.0)
            pv = jnp.dot(w.astype(BF), vx, preferred_element_type=F32)
            if diagonal:
                acc[h, pl.ds(at, tall), :] = pv
            else:
                acc[h, pl.ds(at, tall), :] += pv
            return carry

        lax.fori_loop(0, heads * per_head, step, 0, unroll=2)

    def attend_back(k):
        @pl.when(s >= k)
        def _():
            attend(s - k, False)

    items = [(g, k) for g in range(4) for k in range(1, n)]
    per = n - 1
    state = {"at": 0}

    def advance(to):
        to = min(to, len(items))
        for i in range(state["at"], to):
            stage1(*items[i])
            if i == per:
                own_send(2)
            if i == 2 * per:
                own_send(3)
            if i > 0:
                stage2(*items[i - 1])
        state["at"] = max(state["at"], to)

    def arrived(g):
        for k in range(1, n):
            stage3(g, k)

    for c in copies[:2]:
        c.wait()
    own_send(0)
    copies[2].wait()
    own_send(1)
    copies[3].wait()

    gain = gain_r[...].reshape(1, width).astype(F32)

    def norm_step(i, carry):
        at = pl.ds(pl.multiple_of(i * 32, 32), 32)
        x = tok[at, :].astype(F32)
        r = lax.rsqrt(jnp.mean(x * x, axis=-1, keepdims=True) + EPS)
        normed[at, :] = (x * r * gain).astype(BF)
        return carry

    def norm_rows(lo, hi):
        lax.fori_loop(lo, hi, norm_step, 0)

    steps = rows // 32
    norm_rows(0, steps // 2)
    advance(1)
    norm_rows(steps // 2, steps)
    for c in copies[4:]:
        c.wait()
    advance(per + 2)
    arrived(0)

    lane = lax.broadcasted_iota(jnp.int32, (rows, LANES), 1)

    kv = jnp.dot(
        normed[...],
        gkv[...].reshape(width, 2 * LANES),
        preferred_element_type=F32,
    ).astype(BF)
    kbuf[s] = kv[:, :LANES]
    vbuf[s] = kv[:, LANES:]

    @pl.when(has_right)
    def _():
        for c in kvcopy(s):
            c.start()

    advance(2 * per + 2)
    arrived(1)

    def q_step(h, carry):
        cols = pl.ds(pl.multiple_of(h * 2 * LANES, 2 * LANES), 2 * LANES)
        q = jnp.dot(normed[...], gq[:, :, cols].reshape(width, 2 * LANES), preferred_element_type=F32)
        for e in range(2):
            one = q[:, e * LANES : (e + 1) * LANES]
            q2[2 * h + e, :rows, :] = jnp.where(lane < QK, one, 0.0).astype(BF)
            q2[2 * h + e, rows:, :] = jnp.where(lane >= QK, one, 0.0).astype(BF)
        return carry

    lax.fori_loop(0, heads // 2, q_step, 0)

    attend(s, True)
    advance(3 * per + 1)
    kv_take(1)
    attend_back(1)
    advance(3 * per + 2)
    arrived(2)

    def glu_step(i, carry):
        at = pl.multiple_of(i * 2 * LANES, 2 * LANES)
        cols = pl.ds(at, 2 * LANES)
        cols_gate = pl.ds(pl.multiple_of(chans + at, 2 * LANES), 2 * LANES)
        val = jnp.dot(normed[...], gb[:, :, cols].reshape(width, 2 * LANES), preferred_element_type=F32)
        gate = jnp.dot(
            normed[...], gb[:, :, cols_gate].reshape(width, 2 * LANES), preferred_element_type=F32
        )
        g = (val * jax.nn.sigmoid(gate)).astype(BF)
        gated[:, cols] = g
        pad[RIM:, cols] = g.astype(F32)
        return carry

    lax.fori_loop(0, chans // (2 * LANES), glu_step, 0)

    rim_copy = pltpu.make_async_remote_copy(
        gated.at[pl.ds(rows - RIM, RIM), :],
        rim,
        rims.at[0],
        rims.at[1],
        device_id=right,
        device_id_type=MESH,
    )

    @pl.when(has_right)
    def _():
        rim_copy.start()

    if n > 2:
        kv_take(2)
        attend_back(2)
    advance(len(items))

    @pl.when(has_left)
    def _():
        rim_copy.wait_recv()
        pad[:RIM, :] = rim[...].astype(F32)

    @pl.when(s == 0)
    def _():
        pad[:RIM, :] = jnp.zeros((RIM, chans), F32)

    taps = taps_r.shape[0]
    shift = RIM - (taps - 1)
    tile = min(128, rows)

    def conv_step(i, carry):
        cols = pl.ds(pl.multiple_of(i * LANES, LANES), LANES)
        for r in range(0, rows, tile):
            total = jnp.zeros((tile, LANES), F32)
            for j in range(taps):
                total = total + taps_r[j : j + 1, cols].astype(F32) * pad[
                    r + shift + j : r + shift + j + tile, cols
                ]
            conv[r : r + tile, cols] = total.astype(BF).astype(F32)
        return carry

    lax.fori_loop(0, chans // LANES, conv_step, 0)
    cv = conv[...]
    sq_own[...] = jnp.broadcast_to(jnp.sum(cv * cv, axis=-1, keepdims=True), (rows, LANES))
    sq_copy = pltpu.make_async_remote_copy(
        sq_own, sq_in, sqs.at[0], sqs.at[1], device_id=mate, device_id_type=MESH
    )
    sq_copy.start()

    for k in range(3, n):
        kv_take(k)
        attend_back(k)

    def head_rows(i, carry):
        at = pl.multiple_of(i * tile, tile)
        ids = lax.broadcasted_iota(jnp.int32, (tile, LANES), 1)
        logs = jnp.zeros((tile, LANES), F32)
        for h in range(heads):
            a0 = acc[h, pl.ds(at, tile), :]
            a1 = acc[h, pl.ds(pl.multiple_of(rows + at, tile), tile), :]
            t0, t1 = a0[:, VDIM:], a1[:, VDIM:]
            diff = a0[:, :VDIM] / t0 - lam_r[h] * (a1[:, :VDIM] / t1)
            out = (
                diff
                * lax.rsqrt(jnp.mean(diff * diff, axis=-1, keepdims=True) + EPS)
                * hgain_r[...].astype(F32)
            )
            both[pl.ds(at, tile), h * VDIM : (h + 1) * VDIM] = out.astype(BF)
            logs = jnp.where(ids == 2 * h, jnp.log(t0), logs)
            logs = jnp.where(ids == 2 * h + 1, jnp.log(t1), logs)
        log_r[:, pl.ds(at, tile)] = logs.T[: 2 * heads, :]
        return carry

    lax.fori_loop(0, rows // tile, head_rows, 0)
    stage2(*items[-1])

    sq_copy.wait()
    inv = lax.rsqrt((sq_own[:, :1] + sq_in[:, :1]) / conv_total + EPS)
    cgain = cgain_r[pl.ds(pl.multiple_of(t * chans, LANES), chans)].reshape(1, chans).astype(F32)
    both[:, att_rows:] = jax.nn.silu(conv[...] * inv * cgain).astype(BF)

    def pcopy(o):
        return pltpu.make_async_remote_copy(
            part_out.at[o], part_in.at[o], ps.at[o], pr.at[o], device_id=mate, device_id_type=MESH
        )

    ocols = gc.shape[2]
    mine = pl.ds(pl.multiple_of(t * half, half), half)
    other = pl.ds(pl.multiple_of((1 - t) * half, half), half)

    def out_block(o, _):
        part_out[o] = jnp.dot(both[other, :], gc[o], preferred_element_type=F32).astype(BF)
        pcopy(o).start()
        own = jnp.dot(both[mine, :], gc[o], preferred_element_type=F32)
        keep[o] = own

    out_block(s, None)
    for k in range(1, n):
        stage3(3, k)
        sides(k, out_block)

    def finish(o, carry):
        pcopy(o).wait_recv()
        pcopy(o).wait_send()
        mixed_r[:, pl.ds(pl.multiple_of(o * ocols, ocols), ocols)] = (
            keep[o] + part_in[o].astype(F32)
        ).astype(BF)
        return carry

    lax.fori_loop(0, n, finish, 0)

    for g in range(4):
        drain(g)

    @pl.when(has_right)
    def _():
        rim_copy.wait_send()
        for c in kvcopy(s):
            c.wait_send()

    for k in range(1, n):

        @pl.when((s >= k) & has_right)
        def _():
            for c in kvcopy(s - k):
                c.wait_send()


def body(n, conv_total, tokens, norm_gain, w_query, w_key, w_value, w_gv, w_gg, taps, cgain, hgain, lam, w_out):
    rows, width = tokens.shape
    heads = lam.shape[0]
    chans = w_gv.shape[1]
    qcols = w_query.shape[1]
    wrows = w_query.shape[0]
    ocols = w_out.shape[1]
    half = rows // 2
    any_ = pl.BlockSpec(memory_space=pl.ANY)
    vm = pl.BlockSpec(memory_space=pltpu.VMEM)
    sm = pl.BlockSpec(memory_space=pltpu.SMEM)
    dma = pltpu.SemaphoreType.DMA
    v = pltpu.VMEM
    mixed, logs = pl.pallas_call(
        functools.partial(kernel, n, conv_total),
        out_shape=(
            jax.ShapeDtypeStruct((half, width), BF),
            jax.ShapeDtypeStruct((2 * heads, rows), F32),
        ),
        in_specs=[any_, vm, any_, any_, any_, any_, any_, vm, vm, vm, sm, any_],
        out_specs=(vm, vm),
        scratch_shapes=[
            v((rows, width), BF),
            v((rows, width), BF),
            v((n, wrows, 2 * LANES), BF),
            v((n, wrows, qcols), BF),
            v((n, wrows, 2 * chans), BF),
            v((n, heads * VDIM + chans, ocols), BF),
            v((heads, 2 * rows, LANES), BF),
            v((n, rows, LANES), BF),
            v((n, rows, LANES), BF),
            v((heads, 2 * rows, 2 * VDIM), F32),
            v((rows, chans), BF),
            v((RIM, chans), BF),
            v((rows + RIM, chans), F32),
            v((rows, chans), F32),
            v((rows, LANES), F32),
            v((rows, LANES), F32),
            v((rows, heads * VDIM + chans), BF),
            v((n, half, ocols), BF),
            v((n, half, ocols), BF),
            v((n, half, ocols), F32),
            dma((8,)),
            dma((4, 2, n)),
            dma((4, n)),
            dma((4, n)),
            dma((4, n)),
            dma((4, n)),
            dma((4, n)),
            dma((4, n)),
            dma((4, n)),
            dma((4, n)),
            dma((4, n)),
            dma((2, n)),
            dma((2, n)),
            dma((2,)),
            dma((2,)),
            dma((n,)),
            dma((n,)),
        ],
        compiler_params=pltpu.CompilerParams(
            collective_id=0, has_side_effects=True, vmem_limit_bytes=60 * 1024 * 1024
        ),
    )(
        tokens,
        norm_gain,
        w_query,
        w_key,
        w_value,
        w_gv,
        w_gg,
        taps,
        cgain,
        hgain.reshape(1, -1),
        lam,
        w_out,
    )
    return mixed, logs.T


def solution(mesh):
    n = mesh.shape["sp"]

    def run(*args):
        return body(n, args[8].shape[0], *args)

    return jax.shard_map(
        run,
        mesh=mesh,
        in_specs=(
            P(("fs", "sp"), None),
            P(),
            P("sp", "tp"),
            P("sp", "tp"),
            P("sp", "tp"),
            P("sp", "tp"),
            P("sp", "tp"),
            P(None, "tp"),
            P(),
            P(),
            P("tp"),
            P(None, "sp"),
        ),
        out_specs=(P(("fs", "sp", "tp"), None), P(("fs", "sp"), "tp")),
        check_vma=False,
    )
```

profile of v0, /device:TPU:25, one launch (start us, length us, event | category | flops | bytes accessed | tf_op | source)
XLA Modules:
  0.0 98.0 jit_solution(8298501568618422372)
XLA Ops:
  0.6 94.4 %shard_map.131 = (bf16[256,2048]{1,0:T(8,128)(2,1)}, f32[8,512]{1,0:T(8,128)}) custom-call(bf16[512,2048]{1,0:T(8,128)(2,1)} %tok_h.1, bf16[2048]{0:T(1024)(128)(2,1)} %gain_r.1, bf16[512,512]{1,0:T(8,128)(2,1)} %wq_h.1, bf16[512,128]{1,0:T(8,128)(2,1)} %wk_h.1, bf16[512,128]{1,0:T(8,128)(2,1)} %wv_h.1, bf16[512,512]{1,0:T(8,128)(2,1)} %wgv_h.1, ...), custom_call_target="tpu_custom_call" | custom-call | tf_op jit(solution)/shard_map/pallas_call | solution.py:538
  95.0 0.0 copy-start
  95.1 2.3 %copy.16 = bf16[256,2048]{1,0:T(8,128)(2,1)} copy(bf16[256,2048]{1,0:T(8,128)(2,1)} %get-tuple-element.8) | data formatting | bytes 2097152
  97.4 0.0 copy-done
  97.4 0.6 copy.17
Async XLA Ops:
  95.0 2.3 %copy-start = (f32[8,512]{1,0:T(8,128)S(1)}, f32[8,512]{1,0:T(8,128)}, u32[]{:S(2)}) copy-start(f32[8,512]{1,0:T(8,128)} %get-tuple-element.5) | copy-start | bytes 49156
where the time goes:
time: 98.2 us; the launch traced here: 98 us
  Pallas kernels  94.4 us (96%)
  local copies, waits for them, and re-layouts  2.92 us (3%)
    pallas_call x1, Pallas kernels, body(): pl.pallas_call(functools.partial(kernel, n, conv_total), out_shape=(jax.S...  94.4 us
    unnamed x4, local copies, waits for them, and re-layouts  2.92 us

commit v1 on v0

v1 whole, which is shorter than its diff:
```python
import functools
import math

import jax
import jax.numpy as jnp
from jax import lax
from jax.experimental import pallas as pl
from jax.experimental.pallas import tpu as pltpu
from jax.sharding import PartitionSpec as P

QK = 64
VDIM = 128
EPS = 1e-06
MESH = pl.DeviceIdType.MESH
BF = jnp.bfloat16
F32 = jnp.float32
LANES = 128
RIM = 32
WIDE = 256
TOKEN_CUTS = 4


def kernel(
    n,
    conv_total,
    tok_h,
    gain_r,
    wq_h,
    wk_h,
    wv_h,
    wgv_h,
    wgg_h,
    taps_r,
    cgain_r,
    hgain_r,
    lam_r,
    wo_h,
    mixed_r,
    log_r,
    tok,
    normed,
    gkv,
    gq,
    gb,
    gc,
    q2,
    kvb,
    acc,
    gated,
    rim,
    pad,
    conv,
    taps_in,
    taps_f,
    lam_in,
    lam_s,
    sq_own,
    sq_in,
    both,
    part_out,
    part_in,
    keep,
    lsrc,
    ldst,
    loc,
    zs,
    pr,
    ys,
    ds,
    dr,
    kzs,
    kzr,
    kds,
    kdr,
    tks,
    tkr,
    rims,
    rimr,
    sqs,
    smalls,
    ps,
    prs,
    ls,
    lr,
):
    s = lax.axis_index("sp")
    f = lax.axis_index("fs")
    t = lax.axis_index("tp")
    fx = f + 1 - 2 * (f % 2)
    fy = (f + 2) % 4
    hx = f % 2
    hy = (f // 2) % 2
    native = t == hx
    guest = t != hx
    ph = jnp.where(native, hy, 1 - hy)

    def dev(sp, fs, tp):
        return {"sp": sp, "fs": fs, "tp": tp}

    left = dev(s - 1, f, t)
    right = dev(s + 1, f, t)
    xdev = dev(s, fx, t)
    mate = dev(s, f, 1 - t)
    ydev = dev(s, fy, 1 - t)
    heads = lam_r.shape[1]
    rows, width = tok.shape
    hr = rows // 2
    nb, chans = gb.shape[0], gated.shape[2] * gb.shape[0]
    nc = gc.shape[0]
    oc = gc.shape[3]
    att_rows = heads * VDIM
    has_left = s > 0
    has_right = s < n - 1
    groups = [(gkv, None), (gq, None)]
    groups += [(gb, i) for i in range(nb)] + [(gc, i) for i in range(nc)]
    first_c = 2 + nb

    def slab(g, o):
        buf, i = groups[g]
        return buf.at[o] if i is None else buf.at[i, o]

    def chunk(g, o, half):
        buf, i = groups[g]
        size = buf.shape[-2] // 2
        at = pl.ds(pl.multiple_of(half * size, size), size)
        return buf.at[o, at, :] if i is None else buf.at[i, o, at, :]

    def remote(src, dst, ss, rs, to):
        return pltpu.make_async_remote_copy(src, dst, ss, rs, device_id=to, device_id_type=MESH)

    loads = {}
    count = [0]

    def load(g, a, b):
        c = pltpu.make_async_copy(a, b, loc.at[count[0]])
        count[0] += 1
        loads.setdefault(g, []).append(c)

    load(0, wk_h, gkv.at[s, :, pl.ds(0, LANES)])
    load(0, wv_h, gkv.at[s, :, pl.ds(LANES, LANES)])
    load(1, wq_h, gq.at[s])
    for i in range(nb):
        load(2 + i, wgv_h.at[:, pl.ds(i * WIDE, WIDE)], gb.at[i, s, :, pl.ds(0, WIDE)])
        load(2 + i, wgg_h.at[:, pl.ds(i * WIDE, WIDE)], gb.at[i, s, :, pl.ds(WIDE, WIDE)])
    for i in range(nc):
        cols = pl.ds(i * oc, oc)
        a_rows = pl.ds(pl.multiple_of(hx * att_rows, att_rows), att_rows)
        c_rows = pl.ds(pl.multiple_of(2 * att_rows + hx * chans, chans), chans)
        load(first_c + i, wo_h.at[a_rows, cols], gc.at[i, s, pl.ds(0, att_rows), :])
        load(first_c + i, wo_h.at[c_rows, cols], gc.at[i, s, pl.ds(att_rows, chans), :])
    my_rows = pl.multiple_of(t * hr, hr)
    tok_load = pltpu.make_async_copy(tok_h.at[pl.ds(my_rows, hr), :], tok.at[pl.ds(0, hr), :], loc.at[count[0]])

    @pl.when(native)
    def _():
        for g in range(2):
            for c in loads[g]:
                c.start()

    tok_load.start()

    @pl.when(native)
    def _():
        for g in range(2, first_c):
            for c in loads[g]:
                c.start()

    for g in range(first_c, len(groups)):
        for c in loads[g]:
            c.start()

    bar = pltpu.get_barrier_semaphore()
    for to in (mate, ydev, dev(s, fx, 0), dev(s, fx, 1)):
        pl.semaphore_signal(bar, 1, device_id=to, device_id_type=MESH)

    @pl.when(has_left)
    def _():
        for e in range(2):
            pl.semaphore_signal(bar, 1, device_id=dev(s - 1, f, e), device_id_type=MESH)

    @pl.when(has_right)
    def _():
        for e in range(2):
            pl.semaphore_signal(bar, 1, device_id=dev(s + 1, f, e), device_id_type=MESH)

    pl.semaphore_wait(bar, 4 + jnp.where(has_left, 2, 0) + jnp.where(has_right, 2, 0))

    cut = hr // TOKEN_CUTS
    swaps = [
        remote(
            tok_h.at[pl.ds(pl.multiple_of(my_rows + i * cut, cut), cut), :],
            tok.at[pl.ds(hr + i * cut, cut), :],
            tks.at[i],
            tkr.at[i],
            xdev,
        )
        for i in range(TOKEN_CUTS)
    ]
    for c in swaps:
        c.start()

    def zcopy(g, o, right_way):
        c = chunk(g, o, hy)
        return remote(c, c, zs.at[g, 0 if right_way else 1, o], pr.at[g, o], right if right_way else left)

    def pcopy(g, o):
        c = chunk(g, o, ph)
        return remote(c, c, ys.at[g, o], pr.at[g, o], ydev)

    def dcopy(g, o, half):
        c = chunk(g, o, half)
        return remote(c, c, ds.at[g, o], dr.at[g, o], mate)

    def own_dcopy(g):
        c = slab(g, s)
        return remote(c, c, ds.at[g, s], dr.at[g, s], mate)

    def sides(k, fn):
        @pl.when(s >= k)
        def _():
            fn(s - k, True)

        @pl.when(s + k < n)
        def _():
            fn(s + k, False)

    def own_send(g):
        @pl.when(native)
        def _():
            for c in loads[g]:
                c.wait()

            @pl.when(has_right)
            def _():
                zcopy(g, s, True).start()

            @pl.when(has_left)
            def _():
                zcopy(g, s, False).start()

            if g < first_c:
                own_dcopy(g).start()

        if g >= first_c:

            @pl.when(guest)
            def _():
                for c in loads[g]:
                    c.wait()

    def primary(g, k):
        def go(o, right_way):
            pcopy(g, o).wait_recv()

            @pl.when(native)
            def _():
                @pl.when(has_right if right_way else has_left)
                def _():
                    zcopy(g, o, right_way).start()

                pcopy(g, o).start()

            dcopy(g, o, ph).start()

        sides(k, go)

    def arrived_one(g, k):
        sides(k, lambda o, _: dcopy(g, o, 1 - ph).wait_recv())

    def arrived_own(g):
        if g < first_c:

            @pl.when(guest)
            def _():
                own_dcopy(g).wait_recv()

    def arrived(g):
        arrived_own(g)
        for k in range(1, n):
            arrived_one(g, k)

    def drain(g):
        @pl.when(native)
        def _():
            @pl.when(has_right)
            def _():
                zcopy(g, s, True).wait_send()

            @pl.when(has_left)
            def _():
                zcopy(g, s, False).wait_send()

            if g < first_c:
                own_dcopy(g).wait_send()

        for k in range(1, n):

            def go(o, right_way):
                @pl.when(native)
                def _():
                    pcopy(g, o).wait_send()

                    @pl.when(has_right if right_way else has_left)
                    def _():
                        zcopy(g, o, right_way).wait_send()

                dcopy(g, o, ph).wait_send()

            sides(k, go)

    def kv_at(j, o, half):
        return kvb.at[j, o, pl.ds(pl.multiple_of(half * hr, hr), hr), :]

    def kv_right(j, o):
        c = kv_at(j, o, t)
        return remote(c, c, kzs.at[j, o], kzr.at[j, o], right)

    def kv_mate(j, o, half):
        c = kv_at(j, o, half)
        return remote(c, c, kds.at[j, o], kdr.at[j, o], mate)

    def kv_send(j, o):
        @pl.when(has_right)
        def _():
            kv_right(j, o).start()

        kv_mate(j, o, t).start()

    def kv_take(j, k):
        @pl.when(s >= k)
        def _():
            kv_right(j, s - k).wait_recv()
            kv_send(j, s - k)

    items = [(g, k) for g in range(len(groups)) for k in range(1, n)]
    per = n - 1
    state = {"at": 0}

    def advance(g, part=1.0):
        to = min(len(items), g * per + math.ceil(part * per - 1e-6))
        for i in range(state["at"], to):
            primary(*items[i])
            if (i + 1) % per == 0 and items[i][0] + 2 < len(groups):
                own_send(items[i][0] + 2)
        state["at"] = max(state["at"], to)

    tall = min(256, hr)
    per_map = hr // tall
    per_head = 2 * per_map

    def attend_part(j, o, diagonal, lo, hi):
        kx = kvb[j, o, :, :LANES]
        vx = jnp.concatenate([kvb[j, o, :, LANES:], jnp.ones((rows, VDIM), BF)], axis=1)

        def step(i, carry):
            h = i // per_head
            at = pl.multiple_of((i % per_head) * tall, tall)
            score = lax.dot_general(
                q2[j, h, pl.ds(at, tall), :],
                kx,
                (((1,), (1,)), ((), ())),
                preferred_element_type=F32,
            )
            w = jnp.exp2(score * (QK**-0.5 * math.log2(math.e)))
            if diagonal:
                pos = t * hr + (at % hr) + lax.broadcasted_iota(jnp.int32, w.shape, 0)
                w = jnp.where(lax.broadcasted_iota(jnp.int32, w.shape, 1) <= pos, w, 0.0)
            pv = jnp.dot(w.astype(BF), vx, preferred_element_type=F32)
            if diagonal:
                acc[j, h, pl.ds(at, tall), :] = pv
            else:
                acc[j, h, pl.ds(at, tall), :] += pv
            return carry

        lax.fori_loop(lo * per_head, hi * per_head, step, 0, unroll=2)

    def attend_self(j, between):
        kv_mate(j, s, 1 - t).wait_recv()
        attend_part(j, s, True, 0, heads // 2)
        between()
        attend_part(j, s, True, heads // 2, heads)

    def attend_back(j, k, between):
        @pl.when(s >= k)
        def _():
            kv_mate(j, s - k, 1 - t).wait_recv()
            attend_part(j, s - k, False, 0, heads // 2)

        between()

        @pl.when(s >= k)
        def _():
            attend_part(j, s - k, False, heads // 2, heads)

    own_send(0)
    own_send(1)
    taps_copy = remote(taps_r, taps_in, smalls.at[0], smalls.at[1], mate)
    lam_copy = remote(lam_r, lam_in, smalls.at[2], smalls.at[3], mate)

    @pl.when(native)
    def _():
        taps_copy.start()
        lam_copy.start()
        taps_f[...] = taps_r[...].astype(F32)
        lam_s[...] = lam_r[...]

    gain = gain_r[...].reshape(1, width).astype(F32)

    def norm_step(i, carry):
        at = pl.ds(pl.multiple_of(i * 32, 32), 32)
        x = tok[at, :].astype(F32)
        r = lax.rsqrt(jnp.mean(x * x, axis=-1, keepdims=True) + EPS)
        normed[at, :] = (x * r * gain).astype(BF)
        return carry

    def norm_rows(lo, hi):
        lax.fori_loop(lo // 32, hi // 32, norm_step, 0)

    def project_kv(j):
        kv = jnp.dot(
            normed[j * hr : (j + 1) * hr, :],
            gkv[...].reshape(width, 2 * LANES),
            preferred_element_type=F32,
        ).astype(BF)
        kvb[j, s, pl.ds(my_rows, hr), :] = kv
        kv_send(j, s)

    lane = lax.broadcasted_iota(jnp.int32, (hr, LANES), 1)

    def project_q(j):
        def q_step(h, carry):
            cols = pl.ds(pl.multiple_of(h * 2 * LANES, 2 * LANES), 2 * LANES)
            q = jnp.dot(
                normed[j * hr : (j + 1) * hr, :],
                gq[:, :, cols].reshape(width, 2 * LANES),
                preferred_element_type=F32,
            )
            for e in range(2):
                one = q[:, e * LANES : (e + 1) * LANES]
                q2[j, 2 * h + e, :hr, :] = jnp.where(lane < QK, one, 0.0).astype(BF)
                q2[j, 2 * h + e, hr:, :] = jnp.where(lane >= QK, one, 0.0).astype(BF)
            return carry

        lax.fori_loop(0, heads // 2, q_step, 0)

    def rim_copy(i, to, e):
        return remote(
            gated.at[i, pl.ds(hr - RIM, RIM), :] if e == 0 else gated.at[i, pl.ds(rows - RIM, RIM), :],
            rim.at[i, e],
            rims.at[i, e],
            rimr.at[i, e],
            to,
        )

    def glu(i):
        for j in range(2):
            at = slice(j * hr, (j + 1) * hr)
            val = jnp.dot(normed[at, :], gb[i, :, :, :WIDE].reshape(width, WIDE), preferred_element_type=F32)
            gate = jnp.dot(normed[at, :], gb[i, :, :, WIDE:].reshape(width, WIDE), preferred_element_type=F32)
            g = (val * jax.nn.sigmoid(gate)).astype(BF)
            gated[i, at, :] = g
            pad[j, RIM:, i * WIDE : (i + 1) * WIDE] = g.astype(F32)
        for e in range(2):

            @pl.when(t == 0)
            def _():
                rim_copy(i, mate, e).start()

            @pl.when((t == 1) & has_right)
            def _():
                rim_copy(i, dev(s + 1, f, 0), e).start()

    taps = taps_r.shape[0]
    shift = RIM - (taps - 1)
    tile = min(128, hr)
    wants_rim = (t == 1) | has_left

    def convolve(i):
        @pl.when(wants_rim)
        def _():
            for e in range(2):
                rim_copy(i, mate, e).wait_recv()
                pad[e, :RIM, i * WIDE : (i + 1) * WIDE] = rim[i, e].astype(F32)

        @pl.when((t == 0) & (s == 0))
        def _():
            pad[:, :RIM, i * WIDE : (i + 1) * WIDE] = jnp.zeros((2, RIM, WIDE), F32)

        def conv_step(m, carry):
            cols = pl.ds(pl.multiple_of(i * WIDE + (m // 2) * LANES, LANES), LANES)
            j = m % 2
            for r in range(0, hr, tile):
                total = jnp.zeros((tile, LANES), F32)
                for p in range(taps):
                    total = total + taps_f[p : p + 1, cols] * pad[j, r + shift + p : r + shift + p + tile, cols]
                conv[pl.ds(pl.multiple_of(j * hr + r, tile), tile), cols] = total.astype(BF).astype(F32)
            return carry

        lax.fori_loop(0, 2 * WIDE // LANES, conv_step, 0)

    sq_copy = remote(sq_own, sq_in, sqs.at[0], sqs.at[1], xdev)

    def square_sums():
        cv = conv[...]
        sums = jnp.broadcast_to(jnp.sum(cv * cv, axis=-1, keepdims=True), (rows, LANES))
        sq_own[...] = sums.T[:8, :]
        sq_copy.start()

    def conv_out():
        sq_copy.wait()
        other = jnp.concatenate([sq_in[:, hr:], sq_in[:, :hr]], axis=1)
        inv = lax.rsqrt((sq_own[...] + other) / conv_total + EPS)
        inv = jnp.broadcast_to(inv[:1, :], (LANES, rows)).T[:, :1]
        cgain = cgain_r[pl.ds(pl.multiple_of(hx * chans, LANES), chans)].reshape(1, chans).astype(F32)
        both[:, att_rows:] = jax.nn.silu(conv[...] * inv * cgain).astype(BF)

    def head_rows(j):
        def go(i, carry):
            at = pl.multiple_of(i * tile, tile)
            ids = lax.broadcasted_iota(jnp.int32, (tile, LANES), 1)
            logs = jnp.zeros((tile, LANES), F32)
            for h in range(heads):
                a0 = acc[j, h, pl.ds(at, tile), :]
                a1 = acc[j, h, pl.ds(pl.multiple_of(hr + at, tile), tile), :]
                t0, t1 = a0[:, VDIM:], a1[:, VDIM:]
                diff = a0[:, :VDIM] / t0 - lam_s[:, h : h + 1] * (a1[:, :VDIM] / t1)
                out = (
                    diff
                    * lax.rsqrt(jnp.mean(diff * diff, axis=-1, keepdims=True) + EPS)
                    * hgain_r[...].astype(F32)
                )
                both[pl.ds(pl.multiple_of(j * hr + at, tile), tile), h * VDIM : (h + 1) * VDIM] = out.astype(BF)
                logs = jnp.where(ids == 2 * h, jnp.log(t0), logs)
                logs = jnp.where(ids == 2 * h + 1, jnp.log(t1), logs)
            lsrc[j, :, pl.ds(at, tile)] = logs.T[: 2 * heads, :]
            return carry

        lax.fori_loop(0, hr // tile, go, 0)

    log_mate = remote(lsrc.at[0], ldst.at[t], ls.at[0], lr.at[t], mate)
    log_x = remote(lsrc.at[1], ldst.at[t], ls.at[1], lr.at[t], dev(s, fx, hx))

    def send_logs():
        log_x.start()

        @pl.when(guest)
        def _():
            log_mate.start()

    def take_logs():
        @pl.when(native)
        def _():
            log_r[:, pl.ds(my_rows, hr)] = lsrc[0]
            remote(lsrc.at[0], ldst.at[1 - t], ls.at[0], lr.at[1 - t], mate).wait_recv()
            log_r[:, pl.ds(pl.multiple_of((1 - t) * hr, hr), hr)] = ldst[1 - t]

        @pl.when(guest)
        def _():
            for e in range(2):
                remote(lsrc.at[1], ldst.at[e], ls.at[1], lr.at[e], mate).wait_recv()
                log_r[:, e * hr : (e + 1) * hr] = ldst[e]
            log_mate.wait_send()

        log_x.wait_send()

    def xcopy(i, o):
        return remote(part_out.at[i, o], part_in.at[i, o], ps.at[i, o], prs.at[i, o], xdev)

    def out_block(i, o):
        part_out[i, o] = jnp.dot(both[hr:, :], gc[i, o], preferred_element_type=F32).astype(BF)
        xcopy(i, o).start()
        keep[i, o] = jnp.dot(both[:hr, :], gc[i, o], preferred_element_type=F32)

    def finish(i):
        def go(o, carry):
            xcopy(i, o).wait_recv()
            xcopy(i, o).wait_send()
            mixed_r[:, pl.ds(pl.multiple_of((o * nc + i) * oc, oc), oc)] = (
                keep[i, o] + part_in[i, o].astype(F32)
            ).astype(BF)
            return carry

        lax.fori_loop(0, n, go, 0)

    def nothing():
        pass

    tok_load.wait()
    norm_rows(0, hr)
    advance(0)
    arrived(0)
    project_kv(0)
    advance(1)
    arrived(1)
    project_q(0)
    attend_self(0, lambda: advance(2, 0.4))
    kv_take(0, 1)
    for i in range(TOKEN_CUTS):
        swaps[i].wait_recv()
        norm_rows(hr + i * cut, hr + (i + 1) * cut)
    project_kv(1)
    project_q(1)
    advance(2, 0.7)
    attend_self(1, nothing)
    advance(2)
    if n > 2:
        kv_take(0, 2)
    kv_take(1, 1)
    attend_back(0, 1, lambda: advance(3, 0.4))
    attend_back(1, 1, lambda: advance(3, 0.7))
    arrived(2)

    @pl.when(guest)
    def _():
        taps_copy.wait_recv()
        lam_copy.wait_recv()
        taps_f[...] = taps_in[...].astype(F32)
        lam_s[...] = lam_in[...]

    glu(0)
    advance(3)
    if n > 2:
        kv_take(1, 2)
        attend_back(0, 2, lambda: advance(4, 0.4))
    for i in range(1, nb):
        arrived(2 + i)
        glu(i)
    if n > 2:
        attend_back(1, 2, lambda: advance(4, 0.7))
    for k in range(3, n):
        kv_take(0, k)
        kv_take(1, k)
    for i in range(nb):
        convolve(i)
    square_sums()
    advance(4)
    for k in range(3, n):
        attend_back(1, k, nothing)
    head_rows(1)
    advance(5, 0.4)
    for k in range(3, n):
        attend_back(0, k, nothing)
    head_rows(0)
    send_logs()
    conv_out()
    own_wait = nothing
    for i in range(nc):
        out_block(i, s)
    for i in range(nc):
        for k in range(1, n):
            advance(first_c + i, k / per)
            arrived_one(first_c + i, k)
            sides(k, lambda o, _: out_block(i, o))
    take_logs()
    for i in range(nc):
        finish(i)

    for g in range(len(groups)):
        drain(g)
    for c in swaps:
        c.wait_send()
    for e in range(2):
        for i in range(nb):

            @pl.when((t == 0) | has_right)
            def _():
                rim_copy(i, mate, e).wait_send()

    @pl.when(native)
    def _():
        taps_copy.wait_send()
        lam_copy.wait_send()

    for j in range(2):
        for k in range(n):

            @pl.when(s >= k)
            def _():
                kv_mate(j, s - k, t).wait_send()

                @pl.when(has_right)
                def _():
                    kv_right(j, s - k).wait_send()


def body(n, conv_total, tokens, norm_gain, w_query, w_key, w_value, w_gv, w_gg, taps, cgain, hgain, lam, w_out):
    rows, width = tokens.shape
    heads = lam.shape[0]
    chans = w_gv.shape[1]
    qcols = w_query.shape[1]
    wrows = w_query.shape[0]
    ocols = w_out.shape[1]
    half = rows // 2
    nb = chans // WIDE
    nc = max(1, ocols // WIDE)
    oc = ocols // nc
    feats = heads * VDIM + chans
    ng = 2 + nb + nc
    any_ = pl.BlockSpec(memory_space=pl.ANY)
    vm = pl.BlockSpec(memory_space=pltpu.VMEM)
    dma = pltpu.SemaphoreType.DMA
    v = pltpu.VMEM
    mixed, logs = pl.pallas_call(
        functools.partial(kernel, n, conv_total),
        out_shape=(
            jax.ShapeDtypeStruct((half, width), BF),
            jax.ShapeDtypeStruct((2 * heads, rows), F32),
        ),
        in_specs=[any_, vm, any_, any_, any_, any_, any_, vm, vm, vm, vm, any_],
        out_specs=(vm, vm),
        scratch_shapes=[
            v((rows, width), BF),
            v((rows, width), BF),
            v((n, wrows, 2 * LANES), BF),
            v((n, wrows, qcols), BF),
            v((nb, n, wrows, 2 * WIDE), BF),
            v((nc, n, feats, oc), BF),
            v((2, heads, 2 * half, LANES), BF),
            v((2, n, rows, 2 * LANES), BF),
            v((2, heads, 2 * half, 2 * VDIM), F32),
            v((nb, rows, WIDE), BF),
            v((nb, 2, RIM, WIDE), BF),
            v((2, RIM + half, chans), F32),
            v((rows, chans), F32),
            v(taps.shape, BF),
            v(taps.shape, F32),
            v((1, heads), F32),
            v((1, heads), F32),
            v((8, rows), F32),
            v((8, rows), F32),
            v((rows, feats), BF),
            v((nc, n, half, oc), BF),
            v((nc, n, half, oc), BF),
            v((nc, n, half, oc), F32),
            v((2, 2 * heads, half), F32),
            v((2, 2 * heads, half), F32),
            dma((4 + 2 * nb + 2 * nc,)),
            dma((ng, 2, n)),
            dma((ng, n)),
            dma((ng, n)),
            dma((ng, n)),
            dma((ng, n)),
            dma((2, n)),
            dma((2, n)),
            dma((2, n)),
            dma((2, n)),
            dma((TOKEN_CUTS,)),
            dma((TOKEN_CUTS,)),
            dma((nb, 2)),
            dma((nb, 2)),
            dma((2,)),
            dma((4,)),
            dma((nc, n)),
            dma((nc, n)),
            dma((2,)),
            dma((2,)),
        ],
        compiler_params=pltpu.CompilerParams(
            collective_id=0, has_side_effects=True, vmem_limit_bytes=60 * 1024 * 1024
        ),
    )(
        tokens,
        norm_gain,
        w_query,
        w_key,
        w_value,
        w_gv,
        w_gg,
        taps,
        cgain,
        hgain.reshape(1, -1),
        lam.reshape(1, -1),
        w_out,
    )
    return mixed, logs.T


def solution(mesh):
    n = mesh.shape["sp"]

    def run(*args):
        return body(n, args[8].shape[0], *args)

    return jax.shard_map(
        run,
        mesh=mesh,
        in_specs=(
            P(("fs", "sp"), None),
            P(),
            P("sp", "tp"),
            P("sp", "tp"),
            P("sp", "tp"),
            P("sp", "tp"),
            P("sp", "tp"),
            P(None, "tp"),
            P(),
            P(),
            P("tp"),
            P(None, "sp"),
        ),
        out_specs=(P(("fs", "sp", "tp"), None), P(("fs", "sp"), "tp")),
        check_vma=False,
    )
```

time: 98.2 us -> 119 us (1.21); the launches traced: 98 us -> 117 us
  Pallas kernels: 94.4 us -> 114 us
    pallas_call x1, Pallas kernels: 94.4 us -> 114 us  [body(): pl.pallas_call(functools.partial(kernel, n, conv_total), out_shape=(jax.S...]
where the time goes in v1:
time: 119 us; the launch traced here: 117 us
  Pallas kernels  114 us (96%)
  local copies, waits for them, and re-layouts  2.92 us (2%)
    pallas_call x1, Pallas kernels, body(): pl.pallas_call(functools.partial(kernel, n, conv_total), out_shape=(jax.S...  114 us
    unnamed x4, local copies, waits for them, and re-layouts  2.92 us

profile of v1, /device:TPU:25, one launch (start us, length us, event | category | flops | bytes accessed | tf_op | source)
XLA Modules:
  0.0 117.5 jit_solution(7085483865038661532)
XLA Ops:
  0.6 113.9 %shard_map.131 = (bf16[256,2048]{1,0:T(8,128)(2,1)}, f32[8,512]{1,0:T(8,128)}) custom-call(bf16[512,2048]{1,0:T(8,128)(2,1)} %tok_h.1, bf16[2048]{0:T(1024)(128)(2,1)} %gain_r.1, bf16[512,512]{1,0:T(8,128)(2,1)} %wq_h.1, bf16[512,128]{1,0:T(8,128)(2,1)} %wk_h.1, bf16[512,128]{1,0:T(8,128)(2,1)} %wv_h.1, bf16[512,512]{1,0:T(8,128)(2,1)} %wgv_h.1, ...), custom_call_target="tpu_custom_call" | custom-call | tf_op jit(solution)/shard_map/pallas_call | solution.py:703
  114.5 0.0 copy-start
  114.6 2.3 %copy.16 = bf16[256,2048]{1,0:T(8,128)(2,1)} copy(bf16[256,2048]{1,0:T(8,128)(2,1)} %get-tuple-element.8) | data formatting | bytes 2097152
  116.9 0.0 copy-done
  116.9 0.6 copy.17
Async XLA Ops:
  114.5 2.3 %copy-start = (f32[8,512]{1,0:T(8,128)S(1)}, f32[8,512]{1,0:T(8,128)}, u32[]{:S(2)}) copy-start(f32[8,512]{1,0:T(8,128)} %get-tuple-element.5) | copy-start | bytes 49156

commit v2 on v0

--- a/solution.py
+++ b/solution.py
@@ -16,6 +16,10 @@
 F32 = jnp.float32
 LANES = 128
 RIM = 32
+LOOK = 2
+LAG = 2
+AT = 0
+WIDE = 256
 
 
 def kernel(
@@ -58,6 +62,8 @@
     loc,
     zs,
     zr,
+    zu,
+    zv,
     xs,
     xr,
     ys,
@@ -88,28 +94,39 @@
     chans = gated.shape[1]
     qcols = wq_h.shape[1]
     half = rows // 2
-    groups = (gkv, gq, gb, gc)
+    nb, nc, oc = gb.shape[0], gc.shape[0], gc.shape[3]
+    groups = [(gkv, None), (gq, None)]
+    groups += [(gb, i) for i in range(nb)] + [(gc, i) for i in range(nc)]
+    first_c = 2 + nb
+    ng = first_c + nc
+    twice = ng - 1
     has_left = s > 0
     has_right = s < n - 1
 
     d_rows = wq_h.shape[0]
     att_rows = heads * VDIM
-    locals_ = [
-        (wk_h, gkv.at[s, :, pl.ds(0, LANES)]),
-        (wv_h, gkv.at[s, :, pl.ds(LANES, LANES)]),
-        (wq_h, gq.at[s]),
-        (tok_h, tok),
-        (wgv_h, gb.at[s, :, pl.ds(0, chans)]),
-        (wgg_h, gb.at[s, :, pl.ds(chans, chans)]),
-        (wo_h.at[pl.ds(t * att_rows, att_rows), :], gc.at[s, pl.ds(0, att_rows), :]),
-        (
-            wo_h.at[pl.ds(2 * att_rows + t * chans, chans), :],
-            gc.at[s, pl.ds(att_rows, chans), :],
-        ),
-    ]
-    copies = [pltpu.make_async_copy(a, b, loc.at[i]) for i, (a, b) in enumerate(locals_)]
-    for c in copies:
+    loads = {}
+    count = [0]
+
+    def load(g, src, dst):
+        c = pltpu.make_async_copy(src, dst, loc.at[count[0]])
+        count[0] += 1
+        loads.setdefault(g, []).append(c)
         c.start()
+
+    load(0, wk_h, gkv.at[s, :, pl.ds(0, LANES)])
+    load(0, wv_h, gkv.at[s, :, pl.ds(LANES, LANES)])
+    load(1, wq_h, gq.at[s])
+    load("tok", tok_h, tok)
+    for i in range(nb):
+        load(2 + i, wgv_h.at[:, pl.ds(i * WIDE, WIDE)], gb.at[i, s, :, pl.ds(0, WIDE)])
+        load(2 + i, wgg_h.at[:, pl.ds(i * WIDE, WIDE)], gb.at[i, s, :, pl.ds(WIDE, WIDE)])
+    for i in range(nc):
+        cols = pl.ds(i * oc, oc)
+        a_rows = pl.ds(pl.multiple_of(t * att_rows, att_rows), att_rows)
+        c_rows = pl.ds(pl.multiple_of(2 * att_rows + t * chans, chans), chans)
+        load(first_c + i, wo_h.at[a_rows, cols], gc.at[i, s, pl.ds(0, att_rows), :])
+        load(first_c + i, wo_h.at[c_rows, cols], gc.at[i, s, pl.ds(att_rows, chans), :])
 
     bar = pltpu.get_barrier_semaphore()
     for dev in (xdev, ydev, mate):
@@ -126,12 +143,13 @@
     pl.semaphore_wait(bar, 3 + jnp.where(has_left, 1, 0) + jnp.where(has_right, 1, 0))
 
     def chunk(g, o, q, part=None):
-        buf = groups[g]
-        size = buf.shape[1] // 4
-        if part is None:
-            return buf.at[o, pl.ds(pl.multiple_of(q * size, size), size), :]
-        size = size // 2
-        return buf.at[o, pl.ds(pl.multiple_of((q * 2 + part) * size, size), size), :]
+        buf, i = groups[g]
+        size = buf.shape[-2] // 4
+        if part is not None:
+            size = size // 2
+            q = q * 2 + part
+        at = pl.ds(pl.multiple_of(q * size, size), size)
+        return buf.at[o, at, :] if i is None else buf.at[i, o, at, :]
 
     def zcopy(g, o, right_way):
         c = chunk(g, o, f)
@@ -170,6 +188,17 @@
 
     fd = 3 - f
 
+    def ucopy(o, right_way):
+        c = chunk(twice, o, fd)
+        return pltpu.make_async_remote_copy(
+            c,
+            c,
+            zu.at[0 if right_way else 1, o],
+            zv.at[o],
+            device_id=right if right_way else left,
+            device_id_type=MESH,
+        )
+
     def sides(k, fn):
         @pl.when(s >= k)
         def _():
@@ -180,13 +209,20 @@
             fn(s + k, False)
 
     def own_send(g):
+        for c in loads[g]:
+            c.wait()
+
         @pl.when(has_right)
         def _():
             zcopy(g, s, True).start()
+            if g == twice:
+                ucopy(s, True).start()
 
         @pl.when(has_left)
         def _():
             zcopy(g, s, False).start()
+            if g == twice:
+                ucopy(s, False).start()
 
     def stage1(g, k):
         def go(o, right_way):
@@ -198,9 +234,19 @@
             def _():
                 zcopy(g, o, right_way).start()
 
+            if g == twice:
+                ucopy(o, right_way).wait_recv()
+
+                @pl.when(has_right if right_way else has_left)
+                def _():
+                    ucopy(o, right_way).start()
+
         sides(k, go)
 
     def stage2(g, k):
+        if g == twice:
+            return
+
         def go(o, right_way):
             xcopy(g, o, fx).wait_recv()
             hycopy(g, o, fx).start()
@@ -211,33 +257,42 @@
 
     def stage3(g, k):
         def go(o, right_way):
+            if g == twice:
+                xcopy(g, o, fx).wait_recv()
+                ycopy(g, o, fy).wait_recv()
+                return
             hxcopy(g, o, fd).wait_recv()
             hycopy(g, o, fd).wait_recv()
 
         sides(k, go)
 
     def drain(g):
-        own = zcopy(g, s, True)
-
         @pl.when(has_right)
         def _():
-            own.wait_send()
+            zcopy(g, s, True).wait_send()
+            if g == twice:
+                ucopy(s, True).wait_send()
 
         @pl.when(has_left)
         def _():
             zcopy(g, s, False).wait_send()
+            if g == twice:
+                ucopy(s, False).wait_send()
 
         for k in range(1, n):
 
             def go(o, right_way):
                 xcopy(g, o, f).wait_send()
                 ycopy(g, o, f).wait_send()
-                hycopy(g, o, fx).wait_send()
-                hxcopy(g, o, fy).wait_send()
+                if g != twice:
+                    hycopy(g, o, fx).wait_send()
+                    hxcopy(g, o, fy).wait_send()
 
                 @pl.when(has_right if right_way else has_left)
                 def _():
                     zcopy(g, o, right_way).wait_send()
+                    if g == twice:
+                        ucopy(o, right_way).wait_send()
 
             sides(k, go)
 
@@ -263,7 +318,7 @@
     tall = min(256, rows)
     per_head = 2 * rows // tall
 
-    def attend(o, diagonal):
+    def attend(o, diagonal, lo, hi):
         vx = jnp.concatenate([vbuf[o], jnp.ones((rows, VDIM), BF)], axis=1)
         kx = kbuf[o]
 
@@ -287,39 +342,40 @@
                 acc[h, pl.ds(at, tall), :] += pv
             return carry
 
-        lax.fori_loop(0, heads * per_head, step, 0, unroll=2)
-
-    def attend_back(k):
+        lax.fori_loop(lo * per_head, hi * per_head, step, 0, unroll=2)
+
+    cuts = (0, heads // 2, heads)
+
+    def attend_back(k, e):
         @pl.when(s >= k)
         def _():
-            attend(s - k, False)
-
-    items = [(g, k) for g in range(4) for k in range(1, n)]
+            attend(s - k, False, cuts[e], cuts[e + 1])
+
+    items = [(g, k) for g in range(ng) for k in range(1, n)]
     per = n - 1
     state = {"at": 0}
 
-    def advance(to):
-        to = min(to, len(items))
+    def advance(g, part=1.0):
+        to = min(len(items), g * per + math.ceil(part * per - 1e-6))
         for i in range(state["at"], to):
             stage1(*items[i])
-            if i == per:
-                own_send(2)
-            if i == 2 * per:
-                own_send(3)
-            if i > 0:
-                stage2(*items[i - 1])
+            if i % per == AT and items[i][0] + LOOK < ng:
+                own_send(items[i][0] + LOOK)
+            if i >= LAG:
+                stage2(*items[i - LAG])
+            if i == len(items) - 1:
+                for m in range(LAG):
+                    stage2(*items[i - LAG + 1 + m])
         state["at"] = max(state["at"], to)
 
     def arrived(g):
         for k in range(1, n):
             stage3(g, k)
 
-    for c in copies[:2]:
+    for g in range(LOOK):
+        own_send(g)
+    for c in loads["tok"]:
         c.wait()
-    own_send(0)
-    copies[2].wait()
-    own_send(1)
-    copies[3].wait()
 
     gain = gain_r[...].reshape(1, width).astype(F32)
 
@@ -335,11 +391,9 @@
 
     steps = rows // 32
     norm_rows(0, steps // 2)
-    advance(1)
+    advance(0, 0.3)
     norm_rows(steps // 2, steps)
-    for c in copies[4:]:
-        c.wait()
-    advance(per + 2)
+    advance(1, 0.6)
     arrived(0)
 
     lane = lax.broadcasted_iota(jnp.int32, (rows, LANES), 1)
@@ -357,7 +411,7 @@
         for c in kvcopy(s):
             c.start()
 
-    advance(2 * per + 2)
+    advance(3, 0.3)
     arrived(1)
 
     def q_step(h, carry):
@@ -371,27 +425,13 @@
 
     lax.fori_loop(0, heads // 2, q_step, 0)
 
-    attend(s, True)
-    advance(3 * per + 1)
-    kv_take(1)
-    attend_back(1)
-    advance(3 * per + 2)
-    arrived(2)
-
-    def glu_step(i, carry):
-        at = pl.multiple_of(i * 2 * LANES, 2 * LANES)
-        cols = pl.ds(at, 2 * LANES)
-        cols_gate = pl.ds(pl.multiple_of(chans + at, 2 * LANES), 2 * LANES)
-        val = jnp.dot(normed[...], gb[:, :, cols].reshape(width, 2 * LANES), preferred_element_type=F32)
-        gate = jnp.dot(
-            normed[...], gb[:, :, cols_gate].reshape(width, 2 * LANES), preferred_element_type=F32
-        )
+    def glu(i):
+        cols = slice(i * WIDE, (i + 1) * WIDE)
+        val = jnp.dot(normed[...], gb[i, :, :, :WIDE].reshape(width, WIDE), preferred_element_type=F32)
+        gate = jnp.dot(normed[...], gb[i, :, :, WIDE:].reshape(width, WIDE), preferred_element_type=F32)
         g = (val * jax.nn.sigmoid(gate)).astype(BF)
         gated[:, cols] = g
         pad[RIM:, cols] = g.astype(F32)
-        return carry
-
-    lax.fori_loop(0, chans // (2 * LANES), glu_step, 0)
 
     rim_copy = pltpu.make_async_remote_copy(
         gated.at[pl.ds(rows - RIM, RIM), :],
@@ -401,24 +441,6 @@
         device_id=right,
         device_id_type=MESH,
     )
-
-    @pl.when(has_right)
-    def _():
-        rim_copy.start()
-
-    if n > 2:
-        kv_take(2)
-        attend_back(2)
-    advance(len(items))
-
-    @pl.when(has_left)
-    def _():
-        rim_copy.wait_recv()
-        pad[:RIM, :] = rim[...].astype(F32)
-
-    @pl.when(s == 0)
-    def _():
-        pad[:RIM, :] = jnp.zeros((RIM, chans), F32)
 
     taps = taps_r.shape[0]
     shift = RIM - (taps - 1)
@@ -435,17 +457,8 @@
             conv[r : r + tile, cols] = total.astype(BF).astype(F32)
         return carry
 
-    lax.fori_loop(0, chans // LANES, conv_step, 0)
-    cv = conv[...]
-    sq_own[...] = jnp.broadcast_to(jnp.sum(cv * cv, axis=-1, keepdims=True), (rows, LANES))
-    sq_copy = pltpu.make_async_remote_copy(
-        sq_own, sq_in, sqs.at[0], sqs.at[1], device_id=mate, device_id_type=MESH
-    )
-    sq_copy.start()
-
-    for k in range(3, n):
-        kv_take(k)
-        attend_back(k)
+    def convolve(i):
+        lax.fori_loop(i * WIDE // LANES, (i + 1) * WIDE // LANES, conv_step, 0)
 
     def head_rows(i, carry):
         at = pl.multiple_of(i * tile, tile)
@@ -467,45 +480,103 @@
         log_r[:, pl.ds(at, tile)] = logs.T[: 2 * heads, :]
         return carry
 
+    def pcopy(i, o):
+        return pltpu.make_async_remote_copy(
+            part_out.at[i, o],
+            part_in.at[i, o],
+            ps.at[i, o],
+            pr.at[i, o],
+            device_id=mate,
+            device_id_type=MESH,
+        )
+
+    mine = pl.ds(pl.multiple_of(t * half, half), half)
+    other = pl.ds(pl.multiple_of((1 - t) * half, half), half)
+
+    def out_block(i, o):
+        part_out[i, o] = jnp.dot(both[other, :], gc[i, o], preferred_element_type=F32).astype(BF)
+        pcopy(i, o).start()
+        keep[i, o] = jnp.dot(both[mine, :], gc[i, o], preferred_element_type=F32)
+
+    def finish(i):
+        def go(o, carry):
+            pcopy(i, o).wait_recv()
+            pcopy(i, o).wait_send()
+            mixed_r[:, pl.ds(pl.multiple_of((o * nc + i) * oc, oc), oc)] = (
+                keep[i, o] + part_in[i, o].astype(F32)
+            ).astype(BF)
+            return carry
+
+        lax.fori_loop(0, n, go, 0)
+
+    attend(s, True, 0, heads)
+    advance(4, 0.3)
+    kv_take(1)
+    attend_back(1, 0)
+    attend_back(1, 1)
+    advance(4, 0.6)
+    arrived(2)
+    glu(0)
+    for i in range(1, nb):
+        arrived(2 + i)
+        glu(i)
+
+    @pl.when(has_right)
+    def _():
+        rim_copy.start()
+
+    if n > 2:
+        kv_take(2)
+        attend_back(2, 0)
+        advance(4)
+        attend_back(2, 1)
+    advance(5, 0.3)
+    for k in range(3, n):
+        kv_take(k)
+
+    @pl.when(has_left)
+    def _():
+        rim_copy.wait_recv()
+        pad[:RIM, :] = rim[...].astype(F32)
+
+    @pl.when(s == 0)
+    def _():
+        pad[:RIM, :] = jnp.zeros((RIM, chans), F32)
+
+    for i in range(nb):
+        convolve(i)
+    cv = conv[...]
+    sq_own[...] = jnp.broadcast_to(jnp.sum(cv * cv, axis=-1, keepdims=True), (rows, LANES))
+    sq_copy = pltpu.make_async_remote_copy(
+        sq_own, sq_in, sqs.at[0], sqs.at[1], device_id=mate, device_id_type=MESH
+    )
+    sq_copy.start()
+
+    advance(5, 0.6)
+    for k in range(3, n):
+        attend_back(k, 0)
+        attend_back(k, 1)
+    advance(5)
     lax.fori_loop(0, rows // tile, head_rows, 0)
-    stage2(*items[-1])
-
     sq_copy.wait()
     inv = lax.rsqrt((sq_own[:, :1] + sq_in[:, :1]) / conv_total + EPS)
     cgain = cgain_r[pl.ds(pl.multiple_of(t * chans, LANES), chans)].reshape(1, chans).astype(F32)
     both[:, att_rows:] = jax.nn.silu(conv[...] * inv * cgain).astype(BF)
 
-    def pcopy(o):
-        return pltpu.make_async_remote_copy(
-            part_out.at[o], part_in.at[o], ps.at[o], pr.at[o], device_id=mate, device_id_type=MESH
-        )
-
-    ocols = gc.shape[2]
-    mine = pl.ds(pl.multiple_of(t * half, half), half)
-    other = pl.ds(pl.multiple_of((1 - t) * half, half), half)
-
-    def out_block(o, _):
-        part_out[o] = jnp.dot(both[other, :], gc[o], preferred_element_type=F32).astype(BF)
-        pcopy(o).start()
-        own = jnp.dot(both[mine, :], gc[o], preferred_element_type=F32)
-        keep[o] = own
-
-    out_block(s, None)
+    for i in range(nc):
+        out_block(i, s)
+    for i in range(nc - 1):
+        for k in range(1, n):
+            stage3(first_c + i, k)
+            sides(k, lambda o, _: out_block(i, o))
+    for i in range(nc - 1):
+        finish(i)
     for k in range(1, n):
-        stage3(3, k)
-        sides(k, out_block)
-
-    def finish(o, carry):
-        pcopy(o).wait_recv()
-        pcopy(o).wait_send()
-        mixed_r[:, pl.ds(pl.multiple_of(o * ocols, ocols), ocols)] = (
-            keep[o] + part_in[o].astype(F32)
-        ).astype(BF)
-        return carry
-
-    lax.fori_loop(0, n, finish, 0)
-
-    for g in range(4):
+        stage3(ng - 1, k)
+        sides(k, lambda o, _: out_block(nc - 1, o))
+    finish(nc - 1)
+
+    for g in range(ng):
         drain(g)
 
     @pl.when(has_right)
@@ -530,6 +601,10 @@
     wrows = w_query.shape[0]
     ocols = w_out.shape[1]
     half = rows // 2
+    nb = chans // WIDE
+    nc = max(1, ocols // WIDE)
+    oc = ocols // nc
+    ng = 2 + nb + nc
     any_ = pl.BlockSpec(memory_space=pl.ANY)
     vm = pl.BlockSpec(memory_space=pltpu.VMEM)
     sm = pl.BlockSpec(memory_space=pltpu.SMEM)
@@ -548,8 +623,8 @@
             v((rows, width), BF),
             v((n, wrows, 2 * LANES), BF),
             v((n, wrows, qcols), BF),
-            v((n, wrows, 2 * chans), BF),
-            v((n, heads * VDIM + chans, ocols), BF),
+            v((nb, n, wrows, 2 * WIDE), BF),
+            v((nc, n, heads * VDIM + chans, oc), BF),
             v((heads, 2 * rows, LANES), BF),
             v((n, rows, LANES), BF),
             v((n, rows, LANES), BF),
@@ -561,26 +636,28 @@
             v((rows, LANES), F32),
             v((rows, LANES), F32),
             v((rows, heads * VDIM + chans), BF),
-            v((n, half, ocols), BF),
-            v((n, half, ocols), BF),
-            v((n, half, ocols), F32),
-            dma((8,)),
-            dma((4, 2, n)),
-            dma((4, n)),
-            dma((4, n)),
-            dma((4, n)),
-            dma((4, n)),
-            dma((4, n)),
-            dma((4, n)),
-            dma((4, n)),
-            dma((4, n)),
-            dma((4, n)),
+            v((nc, n, half, oc), BF),
+            v((nc, n, half, oc), BF),
+            v((nc, n, half, oc), F32),
+            dma((4 + 2 * nb + 2 * nc,)),
+            dma((ng, 2, n)),
+            dma((ng, n)),
+            dma((2, n)),
+            dma((n,)),
+            dma((ng, n)),
+            dma((ng, n)),
+            dma((ng, n)),
+            dma((ng, n)),
+            dma((ng, n)),
+            dma((ng, n)),
+            dma((ng, n)),
+            dma((ng, n)),
             dma((2, n)),
             dma((2, n)),
             dma((2,)),
             dma((2,)),
-            dma((n,)),
-            dma((n,)),
+            dma((nc, n)),
+            dma((nc, n)),
         ],
         compiler_params=pltpu.CompilerParams(
             collective_id=0, has_side_effects=True, vmem_limit_bytes=60 * 1024 * 1024

time: 98.2 us -> 95.5 us (0.973)
  Pallas kernels: 94.4 us -> 91.7 us
    pallas_call x1, Pallas kernels: 94.4 us -> 91.7 us  [body(): pl.pallas_call(functools.partial(kernel, n, conv_total), out_shape=(jax.S...]
where the time goes in v2:
time: 95.5 us; the launch traced here: 95.3 us
  Pallas kernels  91.7 us (96%)
  local copies, waits for them, and re-layouts  2.92 us (3%)
    pallas_call x1, Pallas kernels, body(): pl.pallas_call(functools.partial(kernel, n, conv_total), out_shape=(jax.S...  91.7 us
    unnamed x4, local copies, waits for them, and re-layouts  2.92 us

profile of v2, /device:TPU:25, one launch (start us, length us, event | category | flops | bytes accessed | tf_op | source)
XLA Modules:
  0.0 95.3 jit_solution(2899863499344456289)
XLA Ops:
  0.6 91.7 %shard_map.131 = (bf16[256,2048]{1,0:T(8,128)(2,1)}, f32[8,512]{1,0:T(8,128)}) custom-call(bf16[512,2048]{1,0:T(8,128)(2,1)} %tok_h.1, bf16[2048]{0:T(1024)(128)(2,1)} %gain_r.1, bf16[512,512]{1,0:T(8,128)(2,1)} %wq_h.1, bf16[512,128]{1,0:T(8,128)(2,1)} %wk_h.1, bf16[512,128]{1,0:T(8,128)(2,1)} %wv_h.1, bf16[512,512]{1,0:T(8,128)(2,1)} %wgv_h.1, ...), custom_call_target="tpu_custom_call" | custom-call | tf_op jit(solution)/shard_map/pallas_call | solution.py:613
  92.3 0.0 copy-start
  92.3 2.3 %copy.16 = bf16[256,2048]{1,0:T(8,128)(2,1)} copy(bf16[256,2048]{1,0:T(8,128)(2,1)} %get-tuple-element.8) | data formatting | bytes 2097152
  94.7 0.0 copy-done
  94.7 0.6 copy.17
Async XLA Ops:
  92.3 2.3 %copy-start = (f32[8,512]{1,0:T(8,128)S(1)}, f32[8,512]{1,0:T(8,128)}, u32[]{:S(2)}) copy-start(f32[8,512]{1,0:T(8,128)} %get-tuple-element.5) | copy-start | bytes 49156

commit v3 on v2

--- a/solution.py
+++ b/solution.py
@@ -318,6 +318,29 @@
     tall = min(256, rows)
     per_head = 2 * rows // tall
 
+    def attend_self():
+        for r in range(rows // tall):
+            span = (r + 1) * tall
+            vx = jnp.concatenate([vbuf[s, :span, :], jnp.ones((span, VDIM), BF)], axis=1)
+            kx = kbuf[s, :span, :]
+
+            def step(i, carry):
+                h = i // 2
+                at = pl.ds(pl.multiple_of((i % 2) * rows + r * tall, tall), tall)
+                score = lax.dot_general(
+                    q2[h, at, :],
+                    kx,
+                    (((1,), (1,)), ((), ())),
+                    preferred_element_type=F32,
+                )
+                w = jnp.exp2(score * (QK**-0.5 * math.log2(math.e)))
+                pos = r * tall + lax.broadcasted_iota(jnp.int32, w.shape, 0)
+                w = jnp.where(lax.broadcasted_iota(jnp.int32, w.shape, 1) <= pos, w, 0.0)
+                acc[h, at, :] = jnp.dot(w.astype(BF), vx, preferred_element_type=F32)
+                return carry
+
+            lax.fori_loop(0, 2 * heads, step, 0, unroll=2)
+
     def attend(o, diagonal, lo, hi):
         vx = jnp.concatenate([vbuf[o], jnp.ones((rows, VDIM), BF)], axis=1)
         kx = kbuf[o]
@@ -509,7 +532,7 @@
 
         lax.fori_loop(0, n, go, 0)
 
-    attend(s, True, 0, heads)
+    attend_self()
     advance(4, 0.3)
     kv_take(1)
     attend_back(1, 0)

time: 95.5 us -> 95.5 us (level)
  no operation moved by 1% of the time
where the time goes in v3:
time: 95.5 us; the launch traced here: 95.2 us
  Pallas kernels  91.7 us (96%)
  local copies, waits for them, and re-layouts  2.92 us (3%)
    pallas_call x1, Pallas kernels, body(): pl.pallas_call(functools.partial(kernel, n, conv_total), out_shape=(jax.S...  91.7 us
    unnamed x4, local copies, waits for them, and re-layouts  2.92 us

profile of v3, /device:TPU:25, one launch (start us, length us, event | category | flops | bytes accessed | tf_op | source)
XLA Modules:
  0.0 95.2 jit_solution(12174206563059933021)
XLA Ops:
  0.6 91.7 %shard_map.131 = (bf16[256,2048]{1,0:T(8,128)(2,1)}, f32[8,512]{1,0:T(8,128)}) custom-call(bf16[512,2048]{1,0:T(8,128)(2,1)} %tok_h.1, bf16[2048]{0:T(1024)(128)(2,1)} %gain_r.1, bf16[512,512]{1,0:T(8,128)(2,1)} %wq_h.1, bf16[512,128]{1,0:T(8,128)(2,1)} %wk_h.1, bf16[512,128]{1,0:T(8,128)(2,1)} %wv_h.1, bf16[512,512]{1,0:T(8,128)(2,1)} %wgv_h.1, ...), custom_call_target="tpu_custom_call" | custom-call | tf_op jit(solution)/shard_map/pallas_call | solution.py:636
  92.3 0.0 copy-start
  92.3 2.3 %copy.16 = bf16[256,2048]{1,0:T(8,128)(2,1)} copy(bf16[256,2048]{1,0:T(8,128)(2,1)} %get-tuple-element.8) | data formatting | bytes 2097152
  94.6 0.0 copy-done
  94.6 0.6 copy.17
Async XLA Ops:
  92.3 2.3 %copy-start = (f32[8,512]{1,0:T(8,128)S(1)}, f32[8,512]{1,0:T(8,128)}, u32[]{:S(2)}) copy-start(f32[8,512]{1,0:T(8,128)} %get-tuple-element.5) | copy-start | bytes 49156
